TPU v7x, 256 devices: a whole 4x4x8 slice. The times are simulated.
256 devices in a mesh: ep: 64 (over z, x, core), tp: 4 (over y).
Axes of the slice: x: 4, y: 4, z: 8, core: 2. Of those that a mesh axis runs over, the one named last changes fastest.
Arguments:
- conv_input: bfloat16 [65536, 2048], P('ep', 'tp'), may hold values from -6 to 6
- conv_kernel: bfloat16 [31, 2048], P(None, 'tp'), may hold values from -2 to 2
- norm_gain: float32 [2048], P('tp'), may hold values from 0.1 to 1.9
- norm_shift: float32 [2048], P('tp'), may hold values from -3 to 3
- conv_proj: bfloat16 [2048, 2048], P('tp'), may hold values from -0.125 to 0.125
- moe_input: bfloat16 [16384, 2048], P(('ep', 'tp')), may hold values from -6 to 6
- moe_gain: float32 [2048], replicated, may hold values from 0.1 to 1.9
- routes: int32 [16384, 2], P('ep'), may hold values from 0 to 63, all different within a row; in each aligned block of 256 rows (0 to 255, 256 to 511, ...) at most 16 rows name the same one
- route_weights: float32 [16384, 2], P('ep'), may hold values from 0.2 to 1
- gate_proj: bfloat16 [64, 2048, 2048], P('ep', None, 'tp'), may hold values from -0.125 to 0.125
- up_proj: bfloat16 [64, 2048, 2048], P('ep', None, 'tp'), may hold values from -0.125 to 0.125
- down_proj: bfloat16 [64, 2048, 2048], P('ep', 'tp'), may hold values from -0.125 to 0.125
Outputs:
- conv_out: bfloat16 [65536, 2048], P(('ep', 'tp'))
- moe_out: bfloat16 [16384, 2048], P(('ep', 'tp'))
Inputs may be any that keep to these rules, and one draw needn't show every extreme that they name: `routes`: each row names 2 different experts. In each aligned block of 256 rows no expert is named by more than 16 rows, and in some blocks an expert is named by exactly 16 rows.
All inputs are finite; a program needn't handle non-finite values.
Results may differ from a plain program's by a relative error of at most 0.012.
Values may be sent and summed in bfloat16 or wider, within the bound.
A program may use at most 128 MiB of HBM per device.

v0:
```python
import jax
import jax.numpy as jnp
from jax import lax
from jax.sharding import PartitionSpec as P


def shifted(value, axis, steps):
    count = lax.axis_size(axis)
    leading, last = (max(0, -steps), min(count, count - steps))
    return lax.ppermute(value, axis, [(source, source + steps) for source in range(leading, last)])


def laid_out(tiles, dim):
    lengths = list(tiles.shape[1:])
    lengths[dim] *= tiles.shape[0]
    return jnp.moveaxis(tiles, 0, dim).reshape(lengths)


def from_everyone(array, axis):
    size = lax.axis_size(axis)
    return lax.all_to_all(
        jnp.broadcast_to(array[None], (size, *array.shape)), axis, 0, 0, tiled=True
    )


def collect(array, axis, dim):
    return laid_out(from_everyone(array, axis), dim)


def split_up(array, dim, size):
    before, after = (array.shape[:dim], array.shape[dim + 1 :])
    return jnp.moveaxis(array.reshape(*before, size, -1, *after), dim, 0)


def summed_on_arrival(array, axis, dim):
    tiles = split_up(array, dim, lax.axis_size(axis))
    arrived = lax.all_to_all(tiles, axis, split_axis=0, concat_axis=0, tiled=True)
    return arrived.astype(jnp.float32).sum(axis=0)


def local(
    conv_input,
    conv_kernel,
    norm_gain,
    norm_shift,
    conv_proj,
    moe_input,
    moe_gain,
    routes,
    route_weights,
    gate_proj,
    up_proj,
    down_proj,
):
    tp_count = lax.axis_size("tp")
    ep_count = lax.axis_size("ep")
    local_rows, local_width = conv_input.shape
    reach = conv_kernel.shape[0] - 1
    history = shifted(conv_input[local_rows - reach :], "ep", 1)
    padded = jnp.concatenate([history, conv_input], axis=0)
    taps = conv_kernel.astype(jnp.float32)
    mixed = jnp.zeros((local_rows, local_width), jnp.float32)
    for offset in range(reach + 1):
        mixed = mixed + padded[offset : offset + local_rows].astype(jnp.float32) * taps[offset]
    full_width = local_width * tp_count
    sums, squares = lax.psum((jnp.sum(mixed, axis=1), jnp.sum(mixed * mixed, axis=1)), "tp")
    center = sums / full_width
    spread = jnp.maximum(squares / full_width - center * center, 0.0)
    scaled = (mixed - center[:, None]) * lax.rsqrt(spread[:, None] + 1e-05) * norm_gain + norm_shift
    activated = jax.nn.silu(scaled).astype(jnp.bfloat16)
    rows_taken = activated
    conv_out = lax.psum_scatter(
        jnp.dot(rows_taken, conv_proj, preferred_element_type=jnp.float32).astype(jnp.bfloat16),
        "tp",
        scatter_dimension=0,
        tiled=True,
    )
    moe_float = moe_input.astype(jnp.float32)
    normed = (
        moe_float
        * lax.rsqrt(jnp.mean(moe_float * moe_float, axis=1, keepdims=True) + 1e-06)
        * moe_gain
    ).astype(jnp.bfloat16)
    group = collect(normed, "tp", 0)
    group_rows, top_count = routes.shape
    model_width = group.shape[1]
    capacity = 2 * top_count * group_rows // ep_count
    expert_ids = routes.reshape(-1)
    onehot = (expert_ids[:, None] == jnp.arange(ep_count, dtype=jnp.int32)[None, :]).astype(
        jnp.int32
    )
    ranks = jnp.sum((jnp.cumsum(onehot, axis=0) - onehot) * onehot, axis=1)
    targets = ranks * ep_count + expert_ids
    owners = jnp.arange(group_rows * top_count, dtype=jnp.int32) // top_count
    table = jnp.full((capacity * ep_count,), group_rows, jnp.int32).at[targets].set(owners)
    extended = jnp.concatenate([group, jnp.zeros((1, model_width), jnp.bfloat16)], axis=0)
    outgoing = extended[table].reshape(capacity, ep_count, model_width)
    share = capacity // tp_count
    own_slots = lax.dynamic_slice_in_dim(outgoing, lax.axis_index("tp") * share, share, 0)
    landed = lax.all_to_all(own_slots, "ep", split_axis=1, concat_axis=1, tiled=True)
    arrived = lax.all_gather(landed, "tp", axis=0, tiled=True)
    incoming = arrived.reshape(capacity * ep_count, model_width)
    gated = jax.nn.silu(jnp.dot(incoming, gate_proj[0], preferred_element_type=jnp.float32))
    hidden = (gated * jnp.dot(incoming, up_proj[0], preferred_element_type=jnp.float32)).astype(
        jnp.bfloat16
    )
    weights_flat = route_weights.reshape(-1)
    share = capacity // tp_count
    rows_taken = hidden
    totals = summed_on_arrival(
        jnp.dot(rows_taken, down_proj[0], preferred_element_type=jnp.float32).astype(jnp.bfloat16),
        "tp",
        0,
    )
    returned = lax.all_to_all(
        totals.reshape(share, ep_count, model_width).astype(jnp.bfloat16),
        "ep",
        split_axis=1,
        concat_axis=1,
        tiled=True,
    ).astype(jnp.float32)
    local_slot = ranks - lax.axis_index("tp") * share
    inside = (local_slot >= 0) & (local_slot < share)
    position = jnp.clip(local_slot, 0, share - 1) * ep_count + expert_ids
    picked = jnp.where(inside[:, None], returned.reshape(-1, model_width)[position], 0.0)
    combined = jnp.sum(
        (picked * weights_flat[:, None]).reshape(group_rows, top_count, model_width), axis=1
    )
    moe_out = summed_on_arrival(combined.astype(jnp.bfloat16), "tp", 0).astype(jnp.bfloat16)
    return (conv_out, moe_out)


def solution(mesh):
    placed = (
        P("ep", "tp"),
        P(None, "tp"),
        P("tp"),
        P("tp"),
        P("tp", None),
        P(("ep", "tp"), None),
        P(),
        P("ep", None),
        P("ep", None),
        P("ep", None, "tp"),
        P("ep", None, "tp"),
        P("ep", "tp", None),
    )
    return jax.shard_map(
        local,
        mesh=mesh,
        in_specs=placed,
        out_specs=(P(("ep", "tp"), None), P(("ep", "tp"), None)),
        check_vma=False,
    )
```

profile of v0, /device:TPU:8, one launch (start us, length us, event | category | flops | bytes accessed | tf_op | source)
XLA Modules:
  0.0 318.7 jit_solution(13340980202284212392)
XLA Ops:
  7.2 0.0 copy-start
  7.2 0.0 copy-start.4
  7.2 1.3 fusion.43
  8.5 1.1 fusion.45
  9.6 1.1 broadcast_in_dim.15
  10.6 5.6 %all-to-all-start = ((bf16[4,64,2048]{2,1,0:T(8,128)(2,1)}), bf16[4,64,2048]{2,1,0:T(8,128)(2,1)S(1)}, u32[]{:S(2)}, u32[]{:S(2)}) async-start(bf16[4,64,2048]{2,1,0:T(8,128)(2,1)} %broadcast_in_dim.15), calls=%async_computation.1 | async-start | bytes 2097152 | tf_op jit(solution)/shard_map/all_to_all | solution.py:21
  16.3 0.0 all-gather.2.cloned.1.call-start
  16.3 0.0 copy-done.4
  16.3 0.1 copy.46
  16.4 0.1 eq.29
  16.6 0.1 eq.25
  16.7 1.2 reduce-window.6
  18.0 0.2 slice_reduce_fusion
  18.2 0.1 fusion.48
  18.4 0.1 reshape.158
  18.5 2.4 scatter_custom_fusion
  21.0 8.2 %all-to-all-done = bf16[4,64,2048]{2,1,0:T(8,128)(2,1)S(1)} async-done(((bf16[4,64,2048]{2,1,0:T(8,128)(2,1)}), bf16[4,64,2048]{2,1,0:T(8,128)(2,1)S(1)}, u32[]{:S(2)}, u32[]{:S(2)}) %all-to-all-start) | async-done | bytes 1048608 | tf_op jit(solution)/shard_map/all_to_all | solution.py:21
  29.2 0.0 copy-start.1
  29.2 1.0 copy-done.1
  30.2 1.3 concatenate.7
  31.5 6.0 %gather_fusion = bf16[1024,2048]{1,0:T(8,128)(2,1)} fusion(bf16[257,2048]{1,0:T(8,128)(2,1)S(1)} %concatenate.7, s32[1024]{0:T(1024)S(1)} %fusion.50), kind=kCustom, calls=%fused_computation | custom fusion | bytes 8392704 | tf_op jit(solution)/shard_map/gather | solution.py:97
  37.5 1.3 constant_dynamic-slice_fusion
  38.8 0.8 copy.55
  39.6 40.6 %all_to_all.25 = bf16[4,64,2048]{2,0,1:T(4,128)(2,1)S(1)} all-to-all(bf16[4,64,2048]{2,0,1:T(4,128)(2,1)S(1)} %copy.55), channel_id=1, replica_groups=mesh['ep'=64,'tp'=4] {'ep'}, dimensions={1} | all-to-all | bytes 2097152 | tf_op jit(solution)/shard_map/all_to_all | solution.py:100
  80.2 0.0 copy-start.2
  80.2 0.0 copy-start.3
  80.2 1.6 copy.51
  81.8 0.0 copy-start.6
  81.8 0.0 copy-start.7
  81.8 0.0 all-gather.2.cloned.1.call-update
  81.8 0.0 reduce-scatter.2.cloned.1.call-start
  81.8 0.0 copy-done.2
  81.9 1.3 collective-permute-start
  83.2 0.0 copy-done.3
  83.3 0.8 collective-permute-done
  84.0 11.2 %fusion.58 = (f32[1024]{0:T(1024)S(1)}, f32[1024]{0:T(1024)S(1)}, f32[1024,512]{1,0:T(8,128)}) fusion(f32[512]{0:T(512)S(1)} %bitcast.117, bf16[1024,512]{1,0:T(8,128)(2,1)S(1)} %copy-done.2, f32[512]{0:T(512)S(1)} %bitcast.116, bf16[30,512]{1,0:T(8,128)(2,1)S(1)} %collective-permute-done, f32[512]{0:T(512)S(1)} %bitcast.115, f32[512]{0:T(512)S(1)} %bitcast.114, ...), kind=kLoop, calls=%fused_computation.121 | loop fusion | flops 96991232 | bytes 3248128 | tf_op jit(solution)/shard_map/reduce_sum | solution.py:66
  95.2 10.0 %all-reduce.1 = (f32[1024]{0:T(1024)S(1)}, f32[1024]{0:T(1024)S(1)}) all-reduce(f32[1024]{0:T(1024)S(1)} %get-tuple-element.3, f32[1024]{0:T(1024)S(1)} %get-tuple-element.2), channel_id=1, replica_groups=mesh['ep'=64,'tp'=4] {'tp'}, use_global_device_ids=true, to_apply=%region_3.0 | all-reduce | flops 2048 | bytes 16384 | tf_op jit(solution)/shard_map/psum | solution.py:66
  105.2 0.0 copy-done
  105.3 0.0 copy-done.6
  105.3 0.0 copy-done.7
  105.3 6.3 %convolution_convert_fusion.1 = bf16[1024,2048]{1,0:T(8,128)(2,1)} fusion(bf16[512,2048]{1,0:T(8,128)(2,1)S(1)} %copy-done, f32[1024,512]{1,0:T(8,128)} %get-tuple-element.6, f32[512]{0:T(512)S(1)} %copy-done.6, f32[512]{0:T(512)S(1)} %copy-done.7, f32[1024]{0:T(1024)S(1)} %get-tuple-element.39, f32[1024]{0:T(1024)S(1)} %get-tuple-element.38), kind=kOutput, calls=%fused_computation.34 | convolution fusion | flops 2154299392 | bytes 8400896 | tf_op jit(solution)/shard_map/dot_general | solution.py:73
  111.5 0.0 reduce-scatter.2.cloned.1.call-update
  111.6 16.2 %all-gather.2.cloned.1.call-done = bf16[16,64,2048]{2,1,0:T(8,128)(2,1)} async-done(((bf16[4,64,2048]{2,1,0:T(8,128)(2,1)}), bf16[16,64,2048]{2,1,0:T(8,128)(2,1)}) %all-gather.2.cloned.1.call-update) | async-done | bytes 4194320 | tf_op jit(solution)/shard_map/all_gather | solution.py:101
  127.8 6.6 %fusion.1 = f32[1024,512]{1,0:T(8,128)} fusion(bf16[1024,2048]{1,0:T(8,128)(2,1)} %bitcast.119, bf16[1,2048,512]{2,1,0:T(8,128)(2,1)} %param.22), kind=kOutput, calls=%fused_computation.36 | convolution fusion | flops 2147483648 | bytes 8388608 | tf_op jit(solution)/shard_map/dot_general | solution.py:104
  134.3 10.7 %convolution_convert_fusion = bf16[1024,2048]{1,0:T(8,128)(2,1)} fusion(bf16[1,512,2048]{2,1,0:T(8,128)(2,1)} %param.23, f32[1024,512]{1,0:T(8,128)} %fusion.1, bf16[1024,2048]{1,0:T(8,128)(2,1)} %bitcast.120, bf16[1,2048,512]{2,1,0:T(8,128)(2,1)} %param.21), kind=kOutput, calls=%fused_computation.33 | convolution fusion | flops 4300210176 | bytes 14680064 | tf_op jit(solution)/shard_map/dot_general | solution.py:111
  145.0 79.3 %all_to_all.26 = bf16[4,256,2048]{2,1,0:T(8,128)(2,1)} all-to-all(bf16[4,256,2048]{2,1,0:T(8,128)(2,1)} %bitcast.81), channel_id=1, replica_groups=mesh['ep'=64,'tp'=4] {'tp'}, dimensions={0} | all-to-all | bytes 8388608 | tf_op jit(solution)/shard_map/all_to_all | solution.py:37
  224.3 3.1 reduce_sum.73
  227.4 0.0 copy-start.5
  227.4 1.8 copy.52
  229.2 10.7 %all-to-all-start.3 = ((bf16[4,64,2048]{2,0,1:T(4,128)(2,1)}), bf16[4,64,2048]{2,0,1:T(4,128)(2,1)S(1)}, u32[]{:S(2)}, u32[]{:S(2)}) async-start(bf16[4,64,2048]{2,0,1:T(4,128)(2,1)} %copy.52), calls=%async_computation.4 | async-start | bytes 2097152 | tf_op jit(solution)/shard_map/all_to_all | solution.py:115
  239.9 0.2 and.17
  240.0 0.0 copy-done.5
  240.1 0.1 copy.54
  240.2 28.3 %all-to-all-done.3 = bf16[4,64,2048]{2,0,1:T(4,128)(2,1)S(1)} async-done(((bf16[4,64,2048]{2,0,1:T(4,128)(2,1)}), bf16[4,64,2048]{2,0,1:T(4,128)(2,1)S(1)}, u32[]{:S(2)}, u32[]{:S(2)}) %all-to-all-start.3) | async-done | bytes 1048608 | tf_op jit(solution)/shard_map/all_to_all | solution.py:115
  268.5 0.6 copy.53
  269.1 1.7 bitcast_convert_fusion
  270.8 7.0 %gather_fusion.1 = f32[512,2048]{1,0:T(8,128)} fusion(f32[256,2048]{1,0:T(8,128)} %bitcast_convert_fusion, s32[1024]{0:T(1024)S(1)} %pad_clamp_fusion), kind=kCustom, calls=%fused_computation.1 | custom fusion | bytes 8390656 | tf_op jit(solution)/shard_map/gather | solution.py:125
  277.8 5.8 %gather.10 = f32[256,2,2048]{2,1,0:T(2,128)} reshape(f32[512,2048]{1,0:T(8,128)} %gather_fusion.1) | data formatting | bytes 8388608 | tf_op jit(solution)/shard_map/gather | solution.py:125
  283.6 9.9 %multiply_reduce_fusion = bf16[256,2048]{1,0:T(8,128)(2,1)S(1)} fusion(f32[256,2,2048]{2,1,0:T(2,128)} %gather.10, pred[256,2]{1,0:T(8,128)(4,1)S(1)} %and.17, f32[256,2]{1,0:T(8,128)S(1)} %copy.54), kind=kLoop, calls=%fused_computation.32 | loop fusion | flops 2621440 | bytes 5245440 | tf_op jit(solution)/shard_map/reduce_sum | solution.py:126
  293.6 17.3 %all_to_all.27 = bf16[4,64,2048]{2,1,0:T(8,128)(2,1)S(1)} all-to-all(bf16[4,64,2048]{2,1,0:T(8,128)(2,1)S(1)} %bitcast.82), channel_id=1, replica_groups=mesh['ep'=64,'tp'=4] {'tp'}, dimensions={0} | all-to-all | bytes 2097152 | tf_op jit(solution)/shard_map/all_to_all | solution.py:37
  310.9 0.9 reduce_sum.75
  311.8 0.0 reduce-scatter.2.cloned.1.call-done
  (14 shorter events, 0.2 us)
Async XLA Ops:
  7.2 98.1 %copy-start = (bf16[512,2048]{1,0:T(8,128)(2,1)S(1)}, bf16[512,2048]{1,0:T(8,128)(2,1)}, u32[]{:S(2)}) copy-start(bf16[512,2048]{1,0:T(8,128)(2,1)} %param.16) | copy-start | bytes 6291460
  7.2 9.1 %copy-start.4 = (s32[256,2]{0,1:T(2,128)S(1)}, s32[256,2]{0,1:T(2,128)}, u32[]{:S(2)}) copy-start(s32[256,2]{0,1:T(2,128)} %param.19) | copy-start | bytes 6148
  10.6 18.5 %all-to-all-start = ((bf16[4,64,2048]{2,1,0:T(8,128)(2,1)}), bf16[4,64,2048]{2,1,0:T(8,128)(2,1)S(1)}, u32[]{:S(2)}, u32[]{:S(2)}) async-start(bf16[4,64,2048]{2,1,0:T(8,128)(2,1)} %broadcast_in_dim.15), calls=%async_computation.1 | async-start | bytes 2097152 | tf_op jit(solution)/shard_map/all_to_all | solution.py:21
  16.3 111.5 %all-gather.2.cloned.1.call-start = ((), (), s32[]{:S(2)}) async-start(), calls=%async_computation.7 | async-start | bytes 5242880 | tf_op jit(solution)/shard_map/all_gather | solution.py:101
  29.2 1.0 copy-start.1
  80.2 1.6 copy-start.2
  80.2 3.0 copy-start.3
  81.8 23.5 %copy-start.6 = (f32[512]{0:T(512)S(1)}, f32[512]{0:T(512)}, u32[]{:S(2)}) copy-start(f32[512]{0:T(512)} %param.15) | copy-start | bytes 6148
  81.8 23.5 %copy-start.7 = (f32[512]{0:T(512)S(1)}, f32[512]{0:T(512)}, u32[]{:S(2)}) copy-start(f32[512]{0:T(512)} %param.14) | copy-start | bytes 6148
  81.8 230.0 %reduce-scatter.2.cloned.1.call-start = ((), (), s32[]{:S(2)}) async-start(), calls=%async_computation.6 | async-start | bytes 5242880 | tf_op jit(solution)/shard_map/reduce_scatter | solution.py:72
  81.9 2.1 collective-permute-start
  227.4 12.7 %copy-start.5 = (f32[256,2]{0,1:T(2,128)S(1)}, f32[256,2]{0,1:T(2,128)}, u32[]{:S(2)}) copy-start(f32[256,2]{0,1:T(2,128)} %param.20) | copy-start | bytes 6148
  229.2 39.3 %all-to-all-start.3 = ((bf16[4,64,2048]{2,0,1:T(4,128)(2,1)}), bf16[4,64,2048]{2,0,1:T(4,128)(2,1)S(1)}, u32[]{:S(2)}, u32[]{:S(2)}) async-start(bf16[4,64,2048]{2,0,1:T(4,128)(2,1)} %copy.52), calls=%async_computation.4 | async-start | bytes 2097152 | tf_op jit(solution)/shard_map/all_to_all | solution.py:115
Sparse Core Ops, SparseCore 0:
  81.9 45.7 all-gather.1
  130.9 93.0 reduce-scatter.1
where the time goes:
time: 320 us; the launch traced here: 319 us
  blocking collectives  147 us (46%)
  waiting for transfers between devices  53.5 us (17%)
  local copies, waits for them, and re-layouts  31.9 us (10%)
  other arithmetic  30.6 us (10%)
  matrix products  23.5 us (7%)
  starting transfers between devices  17.6 us (6%)
  between operations  14.3 us (4%)
    all_to_all x2, blocking collectives, summed_on_arrival(): lax.all_to_all(tiles, axis, split_axis=0, concat_axis=0, tiled=True)  96.6 us
    all_to_all x1, blocking collectives, local(): lax.all_to_all(own_slots, 'ep', split_axis=1, concat_axis=1, tiled=True)  40.6 us
    all_to_all x1, waiting for transfers between devices, local(): lax.all_to_all(totals.reshape(share, ep_count, model_width).astype(jnp.bf...  28.3 us
    all_gather x1, waiting for transfers between devices, local(): arrived = lax.all_gather(landed, 'tp', axis=0, tiled=True)  16.2 us
    gather x2, local copies, waits for them, and re-layouts, local(): returned.reshape(-1, model_width)[position]  12.8 us
    reduce_sum x1, other arithmetic, local(): jnp.sum(mixed, axis=1)  11.2 us
    dot_general x1, matrix products, local(): jnp.dot(rows_taken, down_proj[0], preferred_element_type=jnp.float32)  10.7 us
    all_to_all x1, starting transfers between devices, local(): lax.all_to_all(totals.reshape(share, ep_count, model_width).astype(jnp.bf...  10.7 us
  transfers between devices with their start and end apart: 5, of which 4 were waited for; matrix products, arithmetic and copies ran while one was open for 22% of the time, Pallas kernels for 0%

commit v1 on v0

v1 whole, which is shorter than its diff:
```python
import jax
import jax.numpy as jnp
from jax import lax
from jax.experimental import pallas as pl
from jax.experimental.pallas import tpu as pltpu
from jax.sharding import PartitionSpec as P

MESH = pl.DeviceIdType.MESH
F32 = jnp.float32
BF16 = jnp.bfloat16

EP = 64
TP = 4
D = 2048
BLK = D // TP
GROUP = 256
TOK = GROUP // TP
CAP = 16
SLOTS = EP * CAP
NCH = 4
CROWS = SLOTS // NCH
CSRC = EP // NCH
HALF = CROWS // 2
ROWS = 1024
QROWS = ROWS // TP
HALO = 32
TAPS = 31
RB = 64
NRB = ROWS // RB
NCB = BLK // 128
OWN = 48


def kernel(
    x_hbm, ck_ref, gain_ref, shift_ref, proj_hbm, mi_hbm, mgain_ref, rt_ref, rw_ref, wg_hbm, wu_hbm, wd_hbm,
    co_hbm, mo_hbm,
    xb, xf, ckf, mixed, tst, act, proj, mi, wg, wu, wd, nrm, grp, dsp, xg, hid, part, ha, hb, fa, fb,
    rout, rin, whi, wlo, cmb, mo, cov,
    load_sem, put_sem, halo_sem, grp_send, grp_recv, st_send, st_recv, dsp_send, dsp_recv,
    ag_send, agl, agr, agfl, agfr, rs_send_sem, hal, hbl, fal, fbl, ret_send, ret_recv, fin_send, fin_recv,
):
    g = lax.axis_index("ep")
    y = lax.axis_index("tp")
    right, left, opp = (y + 1) % TP, (y + 3) % TP, (y + 2) % TP
    z, xx, core = g // 8, (g % 8) // 2, g % 2
    ycol = pl.multiple_of(y * BLK, BLK)

    def offsets(i):
        c, j = i // CSRC, i % CSRC
        p = j % 2
        dz = ((c + 1) % 4) * (1 - p) + (7 - c) * p
        return dz, j // 4, (j // 2) % 2

    def ahead(i):
        dz, dx, dc = offsets(i)
        return ((z + dz) % 8) * 8 + ((xx + dx) % 4) * 2 + (core + dc) % 2

    def behind(i):
        dz, dx, dc = offsets(i)
        return ((z + 8 - dz) % 8) * 8 + ((xx + 4 - dx) % 4) * 2 + (core + dc) % 2

    def remote(src, dst, send, recv, ep, tp):
        return pltpu.make_async_remote_copy(
            src_ref=src, dst_ref=dst, send_sem=send, recv_sem=recv, device_id=(ep, tp), device_id_type=MESH
        )

    def landed(ref, sem):
        pltpu.make_async_copy(ref, ref, sem).wait()

    loads = [
        pltpu.make_async_copy(mi_hbm, mi, load_sem.at[0]),
        pltpu.make_async_copy(x_hbm, xb.at[pl.ds(HALO, ROWS)], load_sem.at[1]),
        pltpu.make_async_copy(proj_hbm, proj, load_sem.at[2]),
        pltpu.make_async_copy(wg_hbm.at[0], wg, load_sem.at[3]),
        pltpu.make_async_copy(wu_hbm.at[0], wu, load_sem.at[4]),
        pltpu.make_async_copy(wd_hbm.at[0], wd, load_sem.at[5]),
    ]
    for load in loads:
        load.start()

    barrier = pltpu.get_barrier_semaphore()
    for d in range(1, TP):
        pl.semaphore_signal(barrier, inc=1, device_id=(g, (y + d) % TP), device_id_type=MESH)

    def greet(s, carry):
        pl.semaphore_signal(barrier, inc=1, device_id=(ahead(s + s // OWN), y), device_id_type=MESH)
        return carry

    lax.fori_loop(0, EP - 1, greet, 0)

    loads[0].wait()
    rows = mi[...].astype(F32)
    scale = lax.rsqrt(jnp.mean(rows * rows, axis=1, keepdims=True) + 1e-6)
    nrm[...] = (rows * scale * mgain_ref[...]).astype(BF16)
    grp[pl.ds(pl.multiple_of(y * TOK, TOK), TOK), :] = nrm[:, pl.ds(ycol, BLK)]

    loads[1].wait()
    for cb in range(NCB):
        ckf[cb, 0:TAPS, :] = ck_ref[:, cb * 128 : cb * 128 + 128].astype(F32)

    def widen(b, carry):
        r = pl.multiple_of(HALO + b * 64, 32)
        for cb in range(NCB):
            xf[cb, pl.ds(r, 64), :] = xb[pl.ds(r, 64), cb * 128 : cb * 128 + 128].astype(F32)
        return carry

    lax.fori_loop(0, ROWS // 64, widen, 0)

    pl.semaphore_wait(barrier, EP - 1 + TP - 1)

    sends = []
    for d in range(1, TP):
        to = (y + d) % TP
        sends.append(
            remote(
                nrm.at[:, pl.ds(pl.multiple_of(to * BLK, BLK), BLK)],
                grp.at[pl.ds(pl.multiple_of(y * TOK, TOK), TOK), :],
                grp_send.at[d],
                grp_recv.at[d],
                g,
                to,
            )
        )
        sends[-1].start()

    halo = remote(xb.at[pl.ds(ROWS, HALO)], xb.at[pl.ds(0, HALO)], halo_sem.at[0], halo_sem.at[1], (g + 1) % EP, y)

    @pl.when(g < EP - 1)
    def _():
        halo.start()

    lane = lax.broadcasted_iota(jnp.int32, (RB, 128), 1)

    def conv_rows(rb, stats):
        base = pl.multiple_of(rb * RB, RB)
        total = jnp.zeros((RB, 128), F32)
        squares = jnp.zeros((RB, 128), F32)
        for cb in range(NCB):
            acc = jnp.zeros((RB, 128), F32)
            for tap in range(TAPS):
                acc = acc + xf[cb, pl.ds(base + (2 + tap), RB), :] * ckf[cb, tap : tap + 1, :]
            mixed[cb, pl.ds(base, RB), :] = acc
            total = total + acc
            squares = squares + acc * acc
        stats = jnp.where(lane == rb, jnp.sum(total, axis=1, keepdims=True), stats)
        return jnp.where(lane == rb + NRB, jnp.sum(squares, axis=1, keepdims=True), stats)

    stats = lax.fori_loop(1, NRB, conv_rows, jnp.zeros((RB, 128), F32))

    @pl.when(g > 0)
    def _():
        halo.wait_recv()

    @pl.when(g == 0)
    def _():
        xb[0:HALO, :] = jnp.zeros((HALO, BLK), BF16)

    for cb in range(NCB):
        xf[cb, 0:HALO, :] = xb[0:HALO, cb * 128 : cb * 128 + 128].astype(F32)
    stats = conv_rows(0, stats)
    tst[TP] = stats
    stat_sends = []
    for d in range(1, TP):
        to = (y + d) % TP
        stat_sends.append(remote(tst.at[TP], tst.at[y], st_send.at[d], st_recv.at[d], g, to))
        stat_sends[-1].start()

    expert_col = lax.broadcasted_iota(jnp.int32, (EP, GROUP), 0)
    named = (rt_ref[0:1, :] == expert_col) | (rt_ref[1:2, :] == expert_col)
    named_f = jnp.where(named, 1.0, 0.0)
    earlier = lax.broadcasted_iota(jnp.int32, (GROUP, GROUP), 0) < lax.broadcasted_iota(jnp.int32, (GROUP, GROUP), 1)
    rank = jnp.dot(named_f.astype(BF16), jnp.where(earlier, 1.0, 0.0).astype(BF16), preferred_element_type=F32)
    rank = jnp.where(named, rank, -1.0).astype(BF16)
    slot = lax.broadcasted_iota(jnp.int32, (SLOTS, EP), 0)
    spread_rows = jnp.where(slot // CAP == lax.broadcasted_iota(jnp.int32, (SLOTS, EP), 1), 1.0, 0.0).astype(BF16)
    ranks = jnp.dot(spread_rows, rank, preferred_element_type=F32)
    place = (lax.broadcasted_iota(jnp.int32, (SLOTS, GROUP), 0) % CAP).astype(F32)
    chosen = jnp.where(ranks == place, 1.0, 0.0).astype(BF16)
    for d in range(1, TP):
        landed(grp.at[pl.ds(0, TOK), :], grp_recv.at[d])
    dsp[...] = jnp.dot(chosen, grp[...], preferred_element_type=F32).astype(BF16)

    def dispatch(s, carry):
        i = s + s // OWN
        e = ahead(i)
        remote(
            dsp.at[pl.ds(pl.multiple_of(e * CAP, CAP), CAP), :],
            xg.at[pl.ds(pl.multiple_of(i * CAP, CAP), CAP), pl.ds(ycol, BLK)],
            dsp_send,
            dsp_recv.at[i // CSRC],
            e,
            y,
        ).start()
        return carry

    lax.fori_loop(0, EP - 1, dispatch, 0)
    xg[OWN * CAP : OWN * CAP + CAP, pl.ds(ycol, BLK)] = dsp[pl.ds(pl.multiple_of(g * CAP, CAP), CAP), :]

    pick = lax.broadcasted_iota(jnp.int32, (128, GROUP), 0)
    table = jnp.where(pick == 0, rt_ref[0:1, :].astype(F32), 0.0)
    table = jnp.where(pick == 1, rt_ref[1:2, :].astype(F32), table)
    table = jnp.where(pick == 2, rw_ref[0:1, :], table)
    table = jnp.where(pick == 3, rw_ref[1:2, :], table)
    table = jnp.transpose(table)
    expert_lane = lax.broadcasted_iota(jnp.int32, (GROUP, EP), 1).astype(F32)
    first = table[:, 0:1] == expert_lane
    second = table[:, 1:2] == expert_lane
    named_t = jnp.where(first | second, 1.0, 0.0)
    before = lax.broadcasted_iota(jnp.int32, (GROUP, GROUP), 1) < lax.broadcasted_iota(jnp.int32, (GROUP, GROUP), 0)
    rank_t = jnp.dot(jnp.where(before, 1.0, 0.0).astype(BF16), named_t.astype(BF16), preferred_element_type=F32)
    rank_t = jnp.where(first | second, rank_t, -1.0).astype(BF16)
    weight_t = jnp.where(first, table[:, 2:3], 0.0) + jnp.where(second, table[:, 3:4], 0.0)
    weight_hi = weight_t.astype(BF16)
    weight_lo = (weight_t - weight_hi.astype(F32)).astype(BF16)
    slot_lane = lax.broadcasted_iota(jnp.int32, (EP, SLOTS), 1)
    spread_cols = jnp.where(slot_lane // CAP == lax.broadcasted_iota(jnp.int32, (EP, SLOTS), 0), 1.0, 0.0).astype(BF16)
    hit = jnp.dot(rank_t, spread_cols, preferred_element_type=F32) == (
        lax.broadcasted_iota(jnp.int32, (GROUP, SLOTS), 1) % CAP
    ).astype(F32)
    whi[...] = jnp.where(hit, jnp.dot(weight_hi, spread_cols, preferred_element_type=F32), 0.0).astype(BF16)
    wlo[...] = jnp.where(hit, jnp.dot(weight_lo, spread_cols, preferred_element_type=F32), 0.0).astype(BF16)

    for d in range(1, TP):
        landed(tst.at[0], st_recv.at[d])
    means = (tst[TP] + tst[right] + tst[opp] + tst[left]) * (1.0 / D)

    def activate(rb, carry):
        base = pl.multiple_of(rb * RB, RB)
        center = jnp.sum(jnp.where(lane == rb, means, 0.0), axis=1, keepdims=True)
        square = jnp.sum(jnp.where(lane == rb + NRB, means, 0.0), axis=1, keepdims=True)
        inv = lax.rsqrt(jnp.maximum(square - center * center, 0.0) + 1e-5)
        for cb in range(NCB):
            cols = slice(cb * 128, cb * 128 + 128)
            v = (mixed[cb, pl.ds(base, RB), :] - center) * inv * gain_ref[:, cols] + shift_ref[:, cols]
            act[pl.ds(base, RB), cols] = (v / (1.0 + jnp.exp(-v))).astype(BF16)
        return carry

    lax.fori_loop(0, NRB, activate, 0)
    loads[2].wait()

    def rs_pieces(j):
        return (
            (part.at[j, opp, pl.ds(0, HALF)], ha.at[j], hal.at[j], right),
            (part.at[j, opp, pl.ds(HALF, HALF)], hb.at[j], hbl.at[j], left),
            (part.at[j, right, pl.ds(HALF, HALF)], fa.at[j, pl.ds(HALF, HALF)], fal.at[j], right),
            (part.at[j, left, pl.ds(0, HALF)], fb.at[j, pl.ds(0, HALF)], fbl.at[j], left),
            (part.at[j, right, pl.ds(0, HALF)], fa.at[j, pl.ds(0, HALF)], fal.at[j], right),
            (part.at[j, left, pl.ds(HALF, HALF)], fb.at[j, pl.ds(HALF, HALF)], fbl.at[j], left),
        )

    def rs_start(j):
        for src, dst, sem, to in rs_pieces(j)[:4]:
            remote(src, dst, rs_send_sem, sem, g, to).start()

    def rs_middle(j):
        pieces = rs_pieces(j)
        landed(ha.at[j], hal.at[j])
        part[j, right, 0:HALF, :] = (part[j, right, 0:HALF, :].astype(F32) + ha[j].astype(F32)).astype(BF16)
        src, dst, sem, to = pieces[4]
        remote(src, dst, rs_send_sem, sem, g, to).start()
        landed(hb.at[j], hbl.at[j])
        part[j, left, HALF:CROWS, :] = (part[j, left, HALF:CROWS, :].astype(F32) + hb[j].astype(F32)).astype(BF16)
        src, dst, sem, to = pieces[5]
        remote(src, dst, rs_send_sem, sem, g, to).start()

    def rs_total(j):
        landed(fa.at[j], fal.at[j])
        landed(fb.at[j], fbl.at[j])
        return (part[j, y].astype(F32) + fa[j].astype(F32) + fb[j].astype(F32)).astype(BF16)

    def project(c):
        col = pl.multiple_of(c * BLK, BLK)

        def quarter(q, carry):
            r = pl.multiple_of(q * QROWS, QROWS)
            part[c, q] = jnp.dot(act[pl.ds(r, QROWS), :], proj[:, pl.ds(col, BLK)], preferred_element_type=F32).astype(BF16)
            return carry

        lax.fori_loop(0, TP, quarter, 0)
        rs_start(c)

    def conv_end(c):
        col = pl.multiple_of(c * BLK, BLK)
        cov[:, pl.ds(col, BLK)] = rs_total(c)
        pltpu.make_async_copy(cov.at[:, pl.ds(col, BLK)], co_hbm.at[:, pl.ds(col, BLK)], put_sem.at[0]).start()

    def crows(c):
        return pl.ds(pl.multiple_of(c * CROWS, CROWS), CROWS)

    def hrows(c, h):
        return pl.ds(pl.multiple_of(c * CROWS + h * HALF, HALF), HALF)

    def colof(t):
        return pl.ds(pl.multiple_of(t * BLK, BLK), BLK)

    def gather_start(c):
        @pl.when(c == NCH - 1)
        def _():
            landed(xg.at[pl.ds(0, CROWS - CAP), pl.ds(0, BLK)], dsp_recv.at[c])

        @pl.when(c < NCH - 1)
        def _():
            landed(xg.at[pl.ds(0, CROWS), pl.ds(0, BLK)], dsp_recv.at[c])

        block = xg.at[crows(c), colof(y)]
        remote(block, block, ag_send, agl.at[c], g, right).start()
        remote(block, block, ag_send, agr.at[c], g, left).start()

    def gather_forward(c):
        landed(xg.at[crows(c), colof(left)], agl.at[c])
        piece = xg.at[hrows(c, 0), colof(left)]
        remote(piece, piece, ag_send, agfl.at[c], g, right).start()
        landed(xg.at[crows(c), colof(right)], agr.at[c])
        piece = xg.at[hrows(c, 1), colof(right)]
        remote(piece, piece, ag_send, agfr.at[c], g, left).start()

    def experts(c):
        landed(xg.at[hrows(c, 0), colof(opp)], agfl.at[c])
        landed(xg.at[hrows(c, 1), colof(opp)], agfr.at[c])

        def up(n, carry):
            cols = pl.ds(pl.multiple_of(n * 256, 256), 256)
            rows = xg[crows(c), :]
            gate = jnp.dot(rows, wg[:, cols], preferred_element_type=F32)
            value = jnp.dot(rows, wu[:, cols], preferred_element_type=F32)
            hid[:, cols] = (gate / (1.0 + jnp.exp(-gate)) * value).astype(BF16)
            return carry

        lax.fori_loop(0, BLK // 256, up, 0)

        def down(q, carry):
            part[NCH + c, q] = jnp.dot(hid[...], wd[:, colof(q)], preferred_element_type=F32).astype(BF16)
            return carry

        lax.fori_loop(0, TP, down, 0)
        rs_start(NCH + c)

    def give_back(c):
        rout[crows(c), :] = rs_total(NCH + c)

        def one(j, carry):
            i = c * CSRC + j

            @pl.when(i != OWN)
            def _():
                remote(
                    rout.at[pl.ds(pl.multiple_of(i * CAP, CAP), CAP), :],
                    rin.at[pl.ds(pl.multiple_of(g * CAP, CAP), CAP), :],
                    ret_send,
                    ret_recv,
                    behind(i),
                    y,
                ).start()

            return carry

        lax.fori_loop(0, CSRC, one, 0)

        @pl.when(c == NCH - 1)
        def _():
            rin[pl.ds(pl.multiple_of(g * CAP, CAP), CAP), :] = rout[OWN * CAP : OWN * CAP + CAP, :]

    project(0)
    for load in loads[3:]:
        load.wait()

    def step(k, carry):
        @pl.when((k >= 1) & (k <= NCH))
        def _():
            gather_forward(k - 1)

        @pl.when(k < NCH)
        def _():
            gather_start(k)

        @pl.when((k >= 2) & (k <= NCH + 1))
        def _():
            rs_middle(NCH + k - 2)

        @pl.when((k <= 1) | (k == NCH + 1))
        def _():
            rs_middle(k - 3 * (k // 5))

        @pl.when((k >= 1) & (k <= NCH))
        def _():
            experts(k - 1)

        @pl.when((k == 0) | (k >= NCH))
        def _():
            project(1 + (k + 1) // 5 + k // 5)

        @pl.when((k >= 2) & (k <= NCH + 1))
        def _():
            give_back(k - 2)

        @pl.when((k <= 1) | (k == NCH + 1))
        def _():
            conv_end(k - 3 * (k // 5))

        return carry

    lax.fori_loop(0, NCH + 2, step, 0)
    rs_middle(3)

    landed(rin.at[pl.ds(0, SLOTS - CAP), :], ret_recv)
    combined = jnp.dot(whi[...], rin[...], preferred_element_type=F32)
    combined = combined + jnp.dot(wlo[...], rin[...], preferred_element_type=F32)
    cmb[...] = combined.astype(BF16)
    for d in range(1, TP):
        to = (y + d) % TP
        sends.append(
            remote(
                cmb.at[pl.ds(pl.multiple_of(to * TOK, TOK), TOK), :],
                mo.at[:, pl.ds(ycol, BLK)],
                fin_send.at[d],
                fin_recv.at[d],
                g,
                to,
            )
        )
        sends[-1].start()
    mo[:, pl.ds(ycol, BLK)] = cmb[pl.ds(pl.multiple_of(y * TOK, TOK), TOK), :]

    conv_end(3)
    for d in range(1, TP):
        landed(mo.at[:, pl.ds(0, BLK)], fin_recv.at[d])
    out = pltpu.make_async_copy(mo, mo_hbm, put_sem.at[1])
    out.start()

    for send in sends + stat_sends:
        send.wait_send()

    @pl.when(g < EP - 1)
    def _():
        halo.wait_send()

    landed(dsp.at[pl.ds(0, SLOTS - CAP), :], dsp_send)
    landed(rout.at[pl.ds(0, SLOTS - CAP), :], ret_send)
    landed(xg.at[pl.ds(0, 3 * CROWS), :], ag_send)
    landed(part.at[:, pl.ds(0, 3)], rs_send_sem)
    landed(cov, put_sem.at[0])
    out.wait()


def local(
    conv_input, conv_kernel, norm_gain, norm_shift, conv_proj, moe_input, moe_gain, routes, route_weights,
    gate_proj, up_proj, down_proj,
):
    vmem = pl.BlockSpec(memory_space=pltpu.VMEM)
    hbm = pl.BlockSpec(memory_space=pl.ANY)
    dma, jobs = pltpu.SemaphoreType.DMA, 2 * NCH
    v = pltpu.VMEM
    return pl.pallas_call(
        kernel,
        out_shape=(
            jax.ShapeDtypeStruct((QROWS, D), BF16),
            jax.ShapeDtypeStruct((TOK, D), BF16),
        ),
        in_specs=[hbm, vmem, vmem, vmem, hbm, hbm, vmem, vmem, vmem, hbm, hbm, hbm],
        out_specs=(hbm, hbm),
        scratch_shapes=[
            v((HALO + ROWS, BLK), BF16),
            v((NCB, HALO + ROWS, 128), F32),
            v((NCB, 32, 128), F32),
            v((NCB, ROWS, 128), F32),
            v((TP + 1, RB, 128), F32),
            v((ROWS, BLK), BF16),
            v((BLK, D), BF16),
            v((TOK, D), BF16),
            v((D, BLK), BF16),
            v((D, BLK), BF16),
            v((BLK, D), BF16),
            v((TOK, D), BF16),
            v((GROUP, BLK), BF16),
            v((SLOTS, BLK), BF16),
            v((SLOTS, D), BF16),
            v((CROWS, BLK), BF16),
            v((jobs, TP, CROWS, BLK), BF16),
            v((jobs, HALF, BLK), BF16),
            v((jobs, HALF, BLK), BF16),
            v((jobs, CROWS, BLK), BF16),
            v((jobs, CROWS, BLK), BF16),
            v((SLOTS, BLK), BF16),
            v((SLOTS, BLK), BF16),
            v((GROUP, SLOTS), BF16),
            v((GROUP, SLOTS), BF16),
            v((GROUP, BLK), BF16),
            v((TOK, D), BF16),
            v((QROWS, D), BF16),
            dma((6,)),
            dma((2,)),
            dma((2,)),
            dma((TP,)),
            dma((TP,)),
            dma((TP,)),
            dma((TP,)),
            dma,
            dma((NCH,)),
            dma,
            dma((NCH,)),
            dma((NCH,)),
            dma((NCH,)),
            dma((NCH,)),
            dma,
            dma((jobs,)),
            dma((jobs,)),
            dma((jobs,)),
            dma((jobs,)),
            dma,
            dma,
            dma((TP,)),
            dma((TP,)),
        ],
        compiler_params=pltpu.CompilerParams(
            collective_id=0, has_side_effects=True, vmem_limit_bytes=60 * 1024 * 1024
        ),
    )(
        conv_input,
        conv_kernel,
        norm_gain.reshape(1, BLK),
        norm_shift.reshape(1, BLK),
        conv_proj,
        moe_input,
        moe_gain.reshape(1, D),
        routes.T,
        route_weights.T,
        gate_proj,
        up_proj,
        down_proj,
    )


def solution(mesh):
    placed = (
        P("ep", "tp"),
        P(None, "tp"),
        P("tp"),
        P("tp"),
        P("tp", None),
        P(("ep", "tp"), None),
        P(),
        P("ep", None),
        P("ep", None),
        P("ep", None, "tp"),
        P("ep", None, "tp"),
        P("ep", "tp", None),
    )
    return jax.shard_map(
        local,
        mesh=mesh,
        in_specs=placed,
        out_specs=(P(("ep", "tp"), None), P(("ep", "tp"), None)),
        check_vma=False,
    )
```

time: 320 us -> 144 us (0.45)
  blocking collectives: 147 us -> 0 us
  Pallas kernels: 0 us -> 140 us
  waiting for transfers between devices: 53.5 us -> 0 us
  other arithmetic: 30.6 us -> 0 us
  local copies, waits for them, and re-layouts: 31.9 us -> 3.05 us
  matrix products: 23.5 us -> 0 us
  starting transfers between devices: 17.6 us -> 0 us
  between operations: 14.3 us -> 0.65 us
    pallas_call x0 -> x1, Pallas kernels: none -> 140 us  [local(): pl.pallas_call(kernel, out_shape=(jax.ShapeDtypeStruct((QROWS, D), BF16),...]
    all_to_all x3 -> x0, blocking collectives: 137 us -> none  [the longest x2 96.6 us: summed_on_arrival(): lax.all_to_all(tiles, axis, split_axis=0, concat_axis=0, tiled=True)]
    all_to_all x2 -> x0, waiting for transfers between devices: 36.5 us -> none  [the longest x1 28.3 us: local(): lax.all_to_all(totals.reshape(share, ep_count, model_width).astype(jnp.bf...]
    reduce_sum x6 -> x0, other arithmetic: 26.5 us -> none  [the longest x1 11.2 us: local(): jnp.sum(mixed, axis=1)]
    dot_general x3 -> x0, matrix products: 23.5 us -> none  [the longest x1 10.7 us: local(): jnp.dot(rows_taken, down_proj[0], preferred_element_type=jnp.float32)]
    gather x3 -> x0, local copies, waits for them, and re-layouts: 18.8 us -> none  [the longest x2 12.8 us: local(): returned.reshape(-1, model_width)[position]]
    all_to_all x2 -> x0, starting transfers between devices: 16.3 us -> none  [the longest x1 10.7 us: local(): lax.all_to_all(totals.reshape(share, ep_count, model_width).astype(jnp.bf...]
    all_gather x1 -> x0, waiting for transfers between devices: 16.2 us -> none  [local(): arrived = lax.all_gather(landed, 'tp', axis=0, tiled=True)]
  transfers between devices with their start and end apart: 5 -> 0, of which waited for: 4 -> 0; matrix products, arithmetic and copies ran while one was open for 22% -> 0% of each run, Pallas kernels for 0% -> 0%
where the time goes in v1:
time: 144 us
  Pallas kernels  140 us (97%)
  local copies, waits for them, and re-layouts  3.05 us (2%)
    pallas_call x1, Pallas kernels, local(): pl.pallas_call(kernel, out_shape=(jax.ShapeDtypeStruct((QROWS, D), BF16),...  140 us
    unnamed x4, local copies, waits for them, and re-layouts  3.05 us

profile of v1, /device:TPU:8, one launch (start us, length us, event | category | flops | bytes accessed | tf_op | source)
XLA Modules:
  0.0 143.7 jit_solution(10970076796546750627)
XLA Ops:
  0.6 140.0 %shard_map.131 = (bf16[256,2048]{1,0:T(8,128)(2,1)}, bf16[64,2048]{1,0:T(8,128)(2,1)}) custom-call(bf16[1024,512]{1,0:T(8,128)(2,1)} %x_hbm.1, bf16[31,512]{1,0:T(8,128)(2,1)} %ck_ref.1, f32[1,512]{1,0:T(1,128)} %bitcast.6, f32[1,512]{1,0:T(1,128)} %bitcast.7, bf16[512,2048]{1,0:T(8,128)(2,1)} %proj_hbm.1, bf16[64,2048]{1,0:T(8,128)(2,1)} %mi_hbm.1, ...), custom_call_target="tpu_custom_call" | custom-call | tf_op jit(solution)/shard_map/pallas_call | solution.py:453
  140.7 0.0 copy-start
  140.7 2.3 %copy.16 = bf16[256,2048]{1,0:T(8,128)(2,1)} copy(bf16[256,2048]{1,0:T(8,128)(2,1)} %get-tuple-element.4) | data formatting | bytes 2097152
  143.0 0.0 copy-done
  143.0 0.7 copy.17
Async XLA Ops:
  140.7 2.4 %copy-start = (bf16[64,2048]{1,0:T(8,128)(2,1)S(1)}, bf16[64,2048]{1,0:T(8,128)(2,1)}, u32[]{:S(2)}) copy-start(bf16[64,2048]{1,0:T(8,128)(2,1)} %get-tuple-element.5) | copy-start | bytes 786436

commit v2 on v1

v2 whole, which is shorter than its diff:
```python
import jax
import jax.numpy as jnp
from jax import lax
from jax.experimental import pallas as pl
from jax.experimental.pallas import tpu as pltpu
from jax.sharding import PartitionSpec as P

MESH = pl.DeviceIdType.MESH
F32 = jnp.float32
BF16 = jnp.bfloat16

EP = 64
TP = 4
D = 2048
BLK = D // TP
GROUP = 256
TOK = GROUP // TP
CAP = 16
SLOTS = EP * CAP
NCH = 4
CROWS = SLOTS // NCH
CSRC = EP // NCH
HALF = CROWS // 2
ROWS = 1024
QROWS = ROWS // TP
HALO = 32
TAPS = 31
RB = 64
NRB = ROWS // RB
NCB = BLK // 128
PIECE = 64
STEPS_Z = ((1, 6), (3, 4), (2, 5), (0, 7))
OWN = 48


def kernel(
    x_hbm, ck_ref, gain_ref, shift_ref, proj_hbm, mi_hbm, mgain_ref, rt_ref, rw_ref, wg_hbm, wu_hbm, wd_hbm,
    cov, mo,
    xb, xf, ckf, mixed, tst, act, actf, proj, mi, wg, wu, wd, nrm, grp, dsp, xg, hid, part, fa, fb,
    rout, rin, rin2, whi, wlo, cmb, fin,
    load_sem, halo_sem, grp_send, grp_recv, st_send, st_recv, dsp_send, dsp_recv,
    act_send, act_recv, w_send, wy, wxl, wxr, wfl, wfr, wc, ag_send, agl, agr, agfl, agfr, rs_send_sem, fal, fbl, ret_send, ret_recv, ret2_send, ret2_recv, fin_send, fin_recv,
):
    g = lax.axis_index("ep")
    y = lax.axis_index("tp")
    right, left, opp = (y + 1) % TP, (y + 3) % TP, (y + 2) % TP
    z, xx, core = g // 8, (g % 8) // 2, g % 2
    ycol = pl.multiple_of(y * BLK, BLK)

    def offsets(i):
        c, j = i // CSRC, i % CSRC
        return STEPS_Z[c][j % 2], j // 4, (j // 2) % 2

    zbase = [((z + dz) % 8) * 8 for dz in range(8)]
    xbase = [[((xx + dx) % 4) * 2 + (core + dc) % 2 for dc in range(2)] for dx in range(4)]
    others = [i for i in range(EP) if i != OWN]

    def ahead(i):
        dz, dx, dc = offsets(i)
        return zbase[dz] + xbase[dx][dc]

    def behind(i):
        dz, dx, dc = offsets(i)
        return zbase[-dz % 8] + xbase[-dx % 4][dc]

    def remote(src, dst, send, recv, ep, tp):
        return pltpu.make_async_remote_copy(
            src_ref=src, dst_ref=dst, send_sem=send, recv_sem=recv, device_id=(ep, tp), device_id_type=MESH
        )

    def landed(ref, sem):
        pltpu.make_async_copy(ref, ref, sem).wait()

    loads = [
        pltpu.make_async_copy(mi_hbm, mi, load_sem.at[0]),
        pltpu.make_async_copy(x_hbm, xb.at[pl.ds(HALO, ROWS)], load_sem.at[1]),
        pltpu.make_async_copy(proj_hbm, proj.at[pl.ds(ycol, BLK)], load_sem.at[2]),
        pltpu.make_async_copy(wg_hbm.at[0], wg, load_sem.at[3]),
        pltpu.make_async_copy(wu_hbm.at[0], wu, load_sem.at[4]),
        pltpu.make_async_copy(wd_hbm.at[0], wd, load_sem.at[5]),
    ]
    barrier = pltpu.get_barrier_semaphore()
    for d in range(1, TP):
        pl.semaphore_signal(barrier, inc=1, device_id=(g, (y + d) % TP), device_id_type=MESH)

    loads[0].start()
    for i in others:
        pl.semaphore_signal(barrier, inc=1, device_id=(ahead(i), y), device_id_type=MESH)
    for load in loads[1:]:
        load.start()

    loads[0].wait()
    rows = mi[...].astype(F32)
    scale = lax.rsqrt(jnp.mean(rows * rows, axis=1, keepdims=True) + 1e-6)
    nrm[...] = (rows * scale * mgain_ref[...]).astype(BF16)
    grp[pl.ds(pl.multiple_of(y * TOK, TOK), TOK), :] = nrm[:, pl.ds(ycol, BLK)]

    pl.semaphore_wait(barrier, EP - 1 + TP - 1)

    sends = []
    for d in range(1, TP):
        to = (y + d) % TP
        sends.append(
            remote(
                nrm.at[:, pl.ds(pl.multiple_of(to * BLK, BLK), BLK)],
                grp.at[pl.ds(pl.multiple_of(y * TOK, TOK), TOK), :],
                grp_send.at[d],
                grp_recv.at[d],
                g,
                to,
            )
        )
        sends[-1].start()

    xnext, xprev = zbase[0] + xbase[1][0], zbase[0] + xbase[3][0]
    partner = zbase[0] + xbase[0][1]
    shards = [(y + d) % TP for d in range(1, TP)]

    def shard_rows(t, start, count):
        return proj.at[pl.ds(pl.multiple_of(t * BLK + start, PIECE // 2), count)]

    half_at = core * (BLK // 2)
    piece_at = half_at + xx * PIECE
    def share_y():
        loads[2].wait()
        block = shard_rows(y, piece_at, PIECE)
        remote(block, block, w_send, wy.at[0], g, right).start()
        remote(block, block, w_send, wy.at[1], g, left).start()

    def share_yy():
        landed(proj.at[pl.ds(0, PIECE)], wy.at[0])
        block = shard_rows(left, piece_at, PIECE // 2)
        remote(block, block, w_send, wy.at[2], g, right).start()
        landed(proj.at[pl.ds(0, PIECE)], wy.at[1])
        block = shard_rows(right, piece_at + PIECE // 2, PIECE // 2)
        remote(block, block, w_send, wy.at[3], g, left).start()

    def share_x():
        landed(proj.at[pl.ds(0, PIECE // 2)], wy.at[2])
        landed(proj.at[pl.ds(0, PIECE // 2)], wy.at[3])
        for t in shards:
            block = shard_rows(t, piece_at, PIECE)
            remote(block, block, w_send, wxl, xnext, y).start()
            remote(block, block, w_send, wxr, xprev, y).start()

    def share_xx():
        landed(proj.at[pl.ds(0, 3 * PIECE)], wxl)
        landed(proj.at[pl.ds(0, 3 * PIECE)], wxr)
        for t in shards:
            block = shard_rows(t, half_at + ((xx + 3) % 4) * PIECE, PIECE // 2)
            remote(block, block, w_send, wfl, xnext, y).start()
            block = shard_rows(t, half_at + ((xx + 1) % 4) * PIECE + PIECE // 2, PIECE // 2)
            remote(block, block, w_send, wfr, xprev, y).start()

    def share_core():
        landed(proj.at[pl.ds(0, 3 * PIECE // 2)], wfl)
        landed(proj.at[pl.ds(0, 3 * PIECE // 2)], wfr)
        for t in shards:
            block = shard_rows(t, half_at, BLK // 2)
            remote(block, block, w_send, wc, partner, y).start()

    loads[1].wait()
    halo = remote(xb.at[pl.ds(ROWS, HALO)], xb.at[pl.ds(0, HALO)], halo_sem.at[0], halo_sem.at[1], (g + 1) % EP, y)

    @pl.when(g < EP - 1)
    def _():
        halo.start()

    expert_col = lax.broadcasted_iota(jnp.int32, (EP, GROUP), 0)
    named = (rt_ref[0:1, :] == expert_col) | (rt_ref[1:2, :] == expert_col)
    named_f = jnp.where(named, 1.0, 0.0)
    earlier = lax.broadcasted_iota(jnp.int32, (GROUP, GROUP), 0) < lax.broadcasted_iota(jnp.int32, (GROUP, GROUP), 1)
    rank = jnp.dot(named_f.astype(BF16), jnp.where(earlier, 1.0, 0.0).astype(BF16), preferred_element_type=F32)
    rank = jnp.where(named, rank, -1.0).astype(BF16)
    slot = lax.broadcasted_iota(jnp.int32, (SLOTS, EP), 0)
    spread_rows = jnp.where(slot // CAP == lax.broadcasted_iota(jnp.int32, (SLOTS, EP), 1), 1.0, 0.0).astype(BF16)
    ranks = jnp.dot(spread_rows, rank, preferred_element_type=F32)
    place = (lax.broadcasted_iota(jnp.int32, (SLOTS, GROUP), 0) % CAP).astype(F32)
    chosen = jnp.where(ranks == place, 1.0, 0.0).astype(BF16)
    for d in range(1, TP):
        landed(grp.at[pl.ds(0, TOK), :], grp_recv.at[d])
    dsp[...] = jnp.dot(chosen, grp[...], preferred_element_type=F32).astype(BF16)

    def dispatch(c):
        for i in range(c * CSRC, c * CSRC + CSRC):
            if i != OWN:
                e = ahead(i)
                remote(
                    dsp.at[pl.ds(pl.multiple_of(e * CAP, CAP), CAP), :],
                    xg.at[pl.ds(i * CAP, CAP), pl.ds(ycol, BLK)],
                    dsp_send,
                    dsp_recv.at[c],
                    e,
                    y,
                ).start()

    dispatch(0)
    share_y()
    xg[OWN * CAP : OWN * CAP + CAP, pl.ds(ycol, BLK)] = dsp[pl.ds(pl.multiple_of(g * CAP, CAP), CAP), :]

    def return_rows(c, source, start, target, send, recv):
        for i in range(c * CSRC, c * CSRC + CSRC):
            if i != OWN:
                remote(
                    source.at[pl.ds(start + (i - c * CSRC) * CAP, CAP), :],
                    target.at[pl.ds(pl.multiple_of(g * CAP, CAP), CAP), :],
                    send,
                    recv,
                    behind(i),
                    y,
                ).start()

    def rs_total(c):
        landed(fa.at[c], fal.at[c])
        landed(fb.at[c], fbl.at[c])
        return (part[c, y].astype(F32) + fa[c].astype(F32) + fb[c].astype(F32)).astype(BF16)

    def crows(c):
        return pl.ds(c * CROWS, CROWS)

    def hrows(c, h):
        return pl.ds(c * CROWS + h * HALF, HALF)

    def colof(t):
        return pl.ds(pl.multiple_of(t * BLK, BLK), BLK)

    def gather_start(c):
        landed(xg.at[pl.ds(0, CROWS - CAP if c == NCH - 1 else CROWS), pl.ds(0, BLK)], dsp_recv.at[c])
        block = xg.at[crows(c), colof(y)]
        remote(block, block, ag_send, agl.at[c], g, right).start()
        remote(block, block, ag_send, agr.at[c], g, left).start()

    def gather_forward(c):
        landed(xg.at[crows(c), colof(left)], agl.at[c])
        piece = xg.at[hrows(c, 0), colof(left)]
        remote(piece, piece, ag_send, agfl.at[c], g, right).start()
        landed(xg.at[crows(c), colof(right)], agr.at[c])
        piece = xg.at[hrows(c, 1), colof(right)]
        remote(piece, piece, ag_send, agfr.at[c], g, left).start()

    def experts(c):
        landed(xg.at[hrows(c, 0), colof(opp)], agfl.at[c])
        landed(xg.at[hrows(c, 1), colof(opp)], agfr.at[c])

        def up(n, carry):
            cols = pl.ds(pl.multiple_of(n * 256, 256), 256)
            rows = xg[crows(c), :]
            gate = jnp.dot(rows, wg[:, cols], preferred_element_type=F32)
            value = jnp.dot(rows, wu[:, cols], preferred_element_type=F32)
            hid[:, cols] = (gate / (1.0 + jnp.exp(-gate)) * value).astype(BF16)
            return carry

        lax.fori_loop(0, BLK // 256, up, 0)

        def down(q):
            part[c, q] = jnp.dot(hid[...], wd[:, colof(q)], preferred_element_type=F32).astype(BF16)

        down(right)
        remote(part.at[c, right], fa.at[c], rs_send_sem, fal.at[c], g, right).start()
        down(left)
        remote(part.at[c, left], fb.at[c], rs_send_sem, fbl.at[c], g, left).start()
        down(opp)
        return_rows(c, part.at[c, opp], 0, rin2, ret2_send, ret2_recv)
        if c == NCH - 1:
            rin2[pl.ds(pl.multiple_of(g * CAP, CAP), CAP), :] = part[c, opp, 0:CAP, :]
        down(y)

    def give_back(c):
        rout[crows(c), :] = rs_total(c)

        return_rows(c, rout, c * CROWS, rin, ret_send, ret_recv)
        if c == NCH - 1:
            rin[pl.ds(pl.multiple_of(g * CAP, CAP), CAP), :] = rout[OWN * CAP : OWN * CAP + CAP, :]

    def conv_out(first, last):
        def columns(n, carry):
            cols = pl.ds(pl.multiple_of(n * 256, 256), 256)
            cov[:, cols] = jnp.dot(actf[...], proj[:, cols], preferred_element_type=F32).astype(BF16)
            return carry

        lax.fori_loop(first, last, columns, 0)

    for cb in range(NCB):
        ckf[cb, 0:TAPS, :] = ck_ref[:, cb * 128 : cb * 128 + 128].astype(F32)

    def widen(b, carry):
        r = pl.multiple_of(HALO + b * 64, 32)
        for cb in range(NCB):
            xf[cb, pl.ds(r, 64), :] = xb[pl.ds(r, 64), cb * 128 : cb * 128 + 128].astype(F32)
        return carry

    lax.fori_loop(0, ROWS // 64, widen, 0)

    lane = lax.broadcasted_iota(jnp.int32, (RB, 128), 1)

    def conv_rows(rb, stats):
        base = pl.multiple_of(rb * RB, RB)
        total = jnp.zeros((RB, 128), F32)
        squares = jnp.zeros((RB, 128), F32)
        for cb in range(NCB):
            acc = jnp.zeros((RB, 128), F32)
            for tap in range(TAPS):
                acc = acc + xf[cb, pl.ds(base + (2 + tap), RB), :] * ckf[cb, tap : tap + 1, :]
            mixed[cb, pl.ds(base, RB), :] = acc
            total = total + acc
            squares = squares + acc * acc
        stats = jnp.where(lane == rb, jnp.sum(total, axis=1, keepdims=True), stats)
        return jnp.where(lane == rb + NRB, jnp.sum(squares, axis=1, keepdims=True), stats)

    stats = lax.fori_loop(1, NRB // 2, conv_rows, jnp.zeros((RB, 128), F32))
    dispatch(1)
    gather_start(0)
    dispatch(2)
    share_yy()
    @pl.when(g > 0)
    def _():
        halo.wait_recv()

    @pl.when(g == 0)
    def _():
        xb[0:HALO, :] = jnp.zeros((HALO, BLK), BF16)

    for cb in range(NCB):
        xf[cb, 0:HALO, :] = xb[0:HALO, cb * 128 : cb * 128 + 128].astype(F32)
    stats = lax.fori_loop(NRB // 2, NRB, conv_rows, stats)
    stats = conv_rows(0, stats)
    tst[TP] = stats
    stat_sends = []
    for d in range(1, TP):
        to = (y + d) % TP
        stat_sends.append(remote(tst.at[TP], tst.at[y], st_send.at[d], st_recv.at[d], g, to))
        stat_sends[-1].start()

    gather_forward(0)
    gather_start(1)
    dispatch(3)
    pick = lax.broadcasted_iota(jnp.int32, (128, GROUP), 0)
    table = jnp.where(pick == 0, rt_ref[0:1, :].astype(F32), 0.0)
    table = jnp.where(pick == 1, rt_ref[1:2, :].astype(F32), table)
    table = jnp.where(pick == 2, rw_ref[0:1, :], table)
    table = jnp.where(pick == 3, rw_ref[1:2, :], table)
    table = jnp.transpose(table)
    expert_lane = lax.broadcasted_iota(jnp.int32, (GROUP, EP), 1).astype(F32)
    first = table[:, 0:1] == expert_lane
    second = table[:, 1:2] == expert_lane
    named_t = jnp.where(first | second, 1.0, 0.0)
    before = lax.broadcasted_iota(jnp.int32, (GROUP, GROUP), 1) < lax.broadcasted_iota(jnp.int32, (GROUP, GROUP), 0)
    rank_t = jnp.dot(jnp.where(before, 1.0, 0.0).astype(BF16), named_t.astype(BF16), preferred_element_type=F32)
    rank_t = jnp.where(first | second, rank_t, -1.0).astype(BF16)
    weight_t = jnp.where(first, table[:, 2:3], 0.0) + jnp.where(second, table[:, 3:4], 0.0)
    weight_hi = weight_t.astype(BF16)
    weight_lo = (weight_t - weight_hi.astype(F32)).astype(BF16)
    slot_lane = lax.broadcasted_iota(jnp.int32, (EP, SLOTS), 1)
    spread_cols = jnp.where(slot_lane // CAP == lax.broadcasted_iota(jnp.int32, (EP, SLOTS), 0), 1.0, 0.0).astype(BF16)
    hit = jnp.dot(rank_t, spread_cols, preferred_element_type=F32) == (
        lax.broadcasted_iota(jnp.int32, (GROUP, SLOTS), 1) % CAP
    ).astype(F32)
    whi[...] = jnp.where(hit, jnp.dot(weight_hi, spread_cols, preferred_element_type=F32), 0.0).astype(BF16)
    wlo[...] = jnp.where(hit, jnp.dot(weight_lo, spread_cols, preferred_element_type=F32), 0.0).astype(BF16)

    for d in range(1, TP):
        landed(tst.at[0], st_recv.at[d])
    means = (tst[TP] + tst[right] + tst[opp] + tst[left]) * (1.0 / D)

    def activate(rb, carry):
        base = pl.multiple_of(rb * RB, RB)
        center = jnp.sum(jnp.where(lane == rb, means, 0.0), axis=1, keepdims=True)
        square = jnp.sum(jnp.where(lane == rb + NRB, means, 0.0), axis=1, keepdims=True)
        inv = lax.rsqrt(jnp.maximum(square - center * center, 0.0) + 1e-5)
        for cb in range(NCB):
            cols = slice(cb * 128, cb * 128 + 128)
            v = (mixed[cb, pl.ds(base, RB), :] - center) * inv * gain_ref[:, cols] + shift_ref[:, cols]
            act[pl.ds(base, RB), cols] = (v / (1.0 + jnp.exp(-v))).astype(BF16)
        return carry

    lax.fori_loop(0, NRB, activate, 0)
    def share_act(d):
        to = (y + d) % TP
        remote(
            act.at[pl.ds(pl.multiple_of(to * QROWS, QROWS), QROWS)],
            actf.at[:, pl.ds(ycol, BLK)],
            act_send,
            act_recv.at[d],
            g,
            to,
        ).start()

    actf[:, pl.ds(ycol, BLK)] = act[pl.ds(pl.multiple_of(y * QROWS, QROWS), QROWS), :]

    for load in loads[3:]:
        load.wait()
    share_x()
    experts(0)
    gather_forward(1)
    gather_start(2)
    give_back(0)
    experts(1)
    gather_forward(2)
    gather_start(3)
    give_back(1)
    experts(2)
    share_xx()
    gather_forward(3)
    give_back(2)
    experts(3)
    share_core()
    give_back(3)
    share_act(2)
    share_act(1)
    share_act(3)

    def combine(rows):
        total = jnp.dot(whi[...], rows[...], preferred_element_type=F32)
        return (total + jnp.dot(wlo[...], rows[...], preferred_element_type=F32)).astype(BF16)

    def to_owners(half):
        for d in (2, 1, 3):
            to = (y + d) % TP
            sends.append(
                remote(
                    cmb.at[half, pl.ds(pl.multiple_of(to * TOK, TOK), TOK), :],
                    fin.at[half, y],
                    fin_send.at[d + 4 * half],
                    fin_recv.at[d + 4 * half],
                    g,
                    to,
                )
            )
            sends[-1].start()
        fin[half, y] = cmb[half, pl.ds(pl.multiple_of(y * TOK, TOK), TOK), :]

    landed(rin2.at[pl.ds(0, SLOTS - CAP), :], ret2_recv)
    cmb[1] = combine(rin2)
    to_owners(1)
    landed(rin.at[pl.ds(0, SLOTS - CAP), :], ret_recv)
    cmb[0] = combine(rin)
    to_owners(0)
    landed(proj.at[pl.ds(0, 3 * (BLK // 2))], wc)
    for d in range(1, TP):
        landed(actf.at[:, pl.ds(0, BLK)], act_recv.at[d])
    conv_out(0, 8)

    for d in range(1, TP):
        landed(fin.at[0, 0], fin_recv.at[d])
        landed(fin.at[0, 0], fin_recv.at[d + 4])
    for t in range(TP):
        both = fin[0, t].astype(F32) + fin[1, (t + 2) % TP].astype(F32)
        mo[:, t * BLK : t * BLK + BLK] = both.astype(BF16)

    for send in sends + stat_sends:
        send.wait_send()

    @pl.when(g < EP - 1)
    def _():
        halo.wait_send()

    landed(dsp.at[pl.ds(0, SLOTS - CAP), :], dsp_send)
    landed(rout.at[pl.ds(0, SLOTS - CAP), :], ret_send)
    landed(xg.at[pl.ds(0, 3 * CROWS), :], ag_send)
    landed(part.at[:, pl.ds(0, 2)], rs_send_sem)
    landed(rout.at[pl.ds(0, SLOTS - CAP), :], ret2_send)
    landed(act.at[pl.ds(0, 3 * QROWS)], act_send)
    landed(proj.at[pl.ds(0, 24 * PIECE)], w_send)


def local(
    conv_input, conv_kernel, norm_gain, norm_shift, conv_proj, moe_input, moe_gain, routes, route_weights,
    gate_proj, up_proj, down_proj,
):
    vmem = pl.BlockSpec(memory_space=pltpu.VMEM)
    hbm = pl.BlockSpec(memory_space=pl.ANY)
    dma, jobs = pltpu.SemaphoreType.DMA, NCH
    v = pltpu.VMEM
    return pl.pallas_call(
        kernel,
        out_shape=(
            pltpu.VMEM((QROWS, D), BF16),
            pltpu.VMEM((TOK, D), BF16),
        ),
        in_specs=[hbm, vmem, vmem, vmem, hbm, hbm, vmem, vmem, vmem, hbm, hbm, hbm],
        out_specs=(vmem, vmem),
        scratch_shapes=[
            v((HALO + ROWS, BLK), BF16),
            v((NCB, HALO + ROWS, 128), F32),
            v((NCB, 32, 128), F32),
            v((NCB, ROWS, 128), F32),
            v((TP + 1, RB, 128), F32),
            v((ROWS, BLK), BF16),
            v((QROWS, D), BF16),
            v((D, D), BF16),
            v((TOK, D), BF16),
            v((D, BLK), BF16),
            v((D, BLK), BF16),
            v((BLK, D), BF16),
            v((TOK, D), BF16),
            v((GROUP, BLK), BF16),
            v((SLOTS, BLK), BF16),
            v((SLOTS, D), BF16),
            v((CROWS, BLK), BF16),
            v((jobs, TP, CROWS, BLK), BF16),
            v((jobs, CROWS, BLK), BF16),
            v((jobs, CROWS, BLK), BF16),
            v((SLOTS, BLK), BF16),
            v((SLOTS, BLK), BF16),
            v((SLOTS, BLK), BF16),
            v((GROUP, SLOTS), BF16),
            v((GROUP, SLOTS), BF16),
            v((2, GROUP, BLK), BF16),
            v((2, TP, TOK, BLK), BF16),
            dma((6,)),
            dma((2,)),
            dma((TP,)),
            dma((TP,)),
            dma((TP,)),
            dma((TP,)),
            dma,
            dma((NCH,)),
            dma,
            dma((TP,)),
            dma,
            dma((TP,)),
            dma,
            dma,
            dma,
            dma,
            dma,
            dma,
            dma((NCH,)),
            dma((NCH,)),
            dma((NCH,)),
            dma((NCH,)),
            dma,
            dma((jobs,)),
            dma((jobs,)),
            dma,
            dma,
            dma,
            dma,
            dma((8,)),
            dma((8,)),
        ],
        compiler_params=pltpu.CompilerParams(
            collective_id=0, has_side_effects=True, vmem_limit_bytes=60 * 1024 * 1024
        ),
    )(
        conv_input,
        conv_kernel,
        norm_gain.reshape(1, BLK),
        norm_shift.reshape(1, BLK),
        conv_proj,
        moe_input,
        moe_gain.reshape(1, D),
        routes.T,
        route_weights.T,
        gate_proj,
        up_proj,
        down_proj,
    )


def solution(mesh):
    placed = (
        P("ep", "tp"),
        P(None, "tp"),
        P("tp"),
        P("tp"),
        P("tp", None),
        P(("ep", "tp"), None),
        P(),
        P("ep", None),
        P("ep", None),
        P("ep", None, "tp"),
        P("ep", None, "tp"),
        P("ep", "tp", None),
    )
    return jax.shard_map(
        local,
        mesh=mesh,
        in_specs=placed,
        out_specs=(P(("ep", "tp"), None), P(("ep", "tp"), None)),
        check_vma=False,
    )
```

time: 144 us -> 116 us (0.81)
  Pallas kernels: 140 us -> 113 us
    pallas_call x1, Pallas kernels: 140 us -> 113 us  [local(): pl.pallas_call(kernel, out_shape=(pltpu.VMEM((QROWS, D), BF16), pltpu.VME...]
    unnamed x4 -> x2, local copies, waits for them, and re-layouts: 3.05 us -> 1.67 us
where the time goes in v2:
time: 116 us; the launch traced here: 115 us
  Pallas kernels  113 us (97%)
  local copies, waits for them, and re-layouts  1.67 us (1%)
    pallas_call x1, Pallas kernels, local(): pl.pallas_call(kernel, out_shape=(pltpu.VMEM((QROWS, D), BF16), pltpu.VME...  113 us

profile of v2, /device:TPU:8, one launch (start us, length us, event | category | flops | bytes accessed | tf_op | source)
XLA Modules:
  0.0 115.4 jit_solution(7140366134631119258)
XLA Ops:
  0.6 113.1 %shard_map.131 = (bf16[256,2048]{1,0:T(8,128)(2,1)S(1)}, bf16[64,2048]{1,0:T(8,128)(2,1)S(1)}) custom-call(bf16[1024,512]{1,0:T(8,128)(2,1)} %x_hbm.1, bf16[31,512]{1,0:T(8,128)(2,1)} %ck_ref.1, f32[1,512]{1,0:T(1,128)} %bitcast.6, f32[1,512]{1,0:T(1,128)} %bitcast.7, bf16[512,2048]{1,0:T(8,128)(2,1)} %proj_hbm.1, bf16[64,2048]{1,0:T(8,128)(2,1)} %mi_hbm.1, ...), custom_call_target="tpu_custom_call" | custom-call | tf_op jit(solution)/shard_map/pallas_call | solution.py:474
  113.7 1.0 copy.16
  114.7 0.7 copy.17

commit v3 on v2

--- a/solution.py
+++ b/solution.py
@@ -17,7 +17,7 @@
 TOK = GROUP // TP
 CAP = 16
 SLOTS = EP * CAP
-NCH = 4
+NCH = 8
 CROWS = SLOTS // NCH
 CSRC = EP // NCH
 HALF = CROWS // 2
@@ -29,8 +29,8 @@
 NRB = ROWS // RB
 NCB = BLK // 128
 PIECE = 64
-STEPS_Z = ((1, 6), (3, 4), (2, 5), (0, 7))
-OWN = 48
+STEPS_Z = (1, 6, 3, 5, 4, 2, 7, 0)
+OWN = 56
 
 
 def kernel(
@@ -49,7 +49,7 @@
 
     def offsets(i):
         c, j = i // CSRC, i % CSRC
-        return STEPS_Z[c][j % 2], j // 4, (j // 2) % 2
+        return STEPS_Z[c], j // 2, j % 2
 
     zbase = [((z + dz) % 8) * 8 for dz in range(8)]
     xbase = [[((xx + dx) % 4) * 2 + (core + dc) % 2 for dc in range(2)] for dx in range(4)]
@@ -195,6 +195,7 @@
                 ).start()
 
     dispatch(0)
+    dispatch(1)
     share_y()
     xg[OWN * CAP : OWN * CAP + CAP, pl.ds(ycol, BLK)] = dsp[pl.ds(pl.multiple_of(g * CAP, CAP), CAP), :]
 
@@ -225,7 +226,7 @@
         return pl.ds(pl.multiple_of(t * BLK, BLK), BLK)
 
     def gather_start(c):
-        landed(xg.at[pl.ds(0, CROWS - CAP if c == NCH - 1 else CROWS), pl.ds(0, BLK)], dsp_recv.at[c])
+        landed(xg.at[pl.ds(0, CROWS - CAP if c == OWN // CSRC else CROWS), pl.ds(0, BLK)], dsp_recv.at[c])
         block = xg.at[crows(c), colof(y)]
         remote(block, block, ag_send, agl.at[c], g, right).start()
         remote(block, block, ag_send, agr.at[c], g, left).start()
@@ -261,7 +262,7 @@
         remote(part.at[c, left], fb.at[c], rs_send_sem, fbl.at[c], g, left).start()
         down(opp)
         return_rows(c, part.at[c, opp], 0, rin2, ret2_send, ret2_recv)
-        if c == NCH - 1:
+        if c == OWN // CSRC:
             rin2[pl.ds(pl.multiple_of(g * CAP, CAP), CAP), :] = part[c, opp, 0:CAP, :]
         down(y)
 
@@ -269,7 +270,7 @@
         rout[crows(c), :] = rs_total(c)
 
         return_rows(c, rout, c * CROWS, rin, ret_send, ret_recv)
-        if c == NCH - 1:
+        if c == OWN // CSRC:
             rin[pl.ds(pl.multiple_of(g * CAP, CAP), CAP), :] = rout[OWN * CAP : OWN * CAP + CAP, :]
 
     def conv_out(first, last):
@@ -308,9 +309,10 @@
         return jnp.where(lane == rb + NRB, jnp.sum(squares, axis=1, keepdims=True), stats)
 
     stats = lax.fori_loop(1, NRB // 2, conv_rows, jnp.zeros((RB, 128), F32))
-    dispatch(1)
+    dispatch(2)
+    dispatch(3)
     gather_start(0)
-    dispatch(2)
+    dispatch(4)
     share_yy()
     @pl.when(g > 0)
     def _():
@@ -333,7 +335,9 @@
 
     gather_forward(0)
     gather_start(1)
-    dispatch(3)
+    dispatch(5)
+    dispatch(6)
+    dispatch(7)
     pick = lax.broadcasted_iota(jnp.int32, (128, GROUP), 0)
     table = jnp.where(pick == 0, rt_ref[0:1, :].astype(F32), 0.0)
     table = jnp.where(pick == 1, rt_ref[1:2, :].astype(F32), table)
@@ -390,21 +394,19 @@
     for load in loads[3:]:
         load.wait()
     share_x()
-    experts(0)
-    gather_forward(1)
-    gather_start(2)
-    give_back(0)
-    experts(1)
-    gather_forward(2)
-    gather_start(3)
-    give_back(1)
-    experts(2)
-    share_xx()
-    gather_forward(3)
-    give_back(2)
-    experts(3)
-    share_core()
-    give_back(3)
+    for k in range(NCH):
+        experts(k)
+        if k + 1 < NCH:
+            gather_forward(k + 1)
+        if k + 2 < NCH:
+            gather_start(k + 2)
+        if k >= 1:
+            give_back(k - 1)
+        if k == NCH - 3:
+            share_xx()
+        if k == NCH - 1:
+            share_core()
+    give_back(NCH - 1)
     share_act(2)
     share_act(1)
     share_act(3)
@@ -456,7 +458,7 @@
 
     landed(dsp.at[pl.ds(0, SLOTS - CAP), :], dsp_send)
     landed(rout.at[pl.ds(0, SLOTS - CAP), :], ret_send)
-    landed(xg.at[pl.ds(0, 3 * CROWS), :], ag_send)
+    landed(xg.at[pl.ds(0, 3 * SLOTS // TP), :], ag_send)
     landed(part.at[:, pl.ds(0, 2)], rs_send_sem)
     landed(rout.at[pl.ds(0, SLOTS - CAP), :], ret2_send)
     landed(act.at[pl.ds(0, 3 * QROWS)], act_send)

time: 116 us -> 113 us (0.974)
  Pallas kernels: 113 us -> 111 us
    pallas_call x1, Pallas kernels: 113 us -> 111 us  [local(): pl.pallas_call(kernel, out_shape=(pltpu.VMEM((QROWS, D), BF16), pltpu.VME...]
where the time goes in v3:
time: 113 us
  Pallas kernels  111 us (98%)
  local copies, waits for them, and re-layouts  1.67 us (1%)
    pallas_call x1, Pallas kernels, local(): pl.pallas_call(kernel, out_shape=(pltpu.VMEM((QROWS, D), BF16), pltpu.VME...  111 us

profile of v3, /device:TPU:8, one launch (start us, length us, event | category | flops | bytes accessed | tf_op | source)
XLA Modules:
  0.0 112.9 jit_solution(9598397319690794205)
XLA Ops:
  0.6 110.6 %shard_map.131 = (bf16[256,2048]{1,0:T(8,128)(2,1)S(1)}, bf16[64,2048]{1,0:T(8,128)(2,1)S(1)}) custom-call(bf16[1024,512]{1,0:T(8,128)(2,1)} %x_hbm.1, bf16[31,512]{1,0:T(8,128)(2,1)} %ck_ref.1, f32[1,512]{1,0:T(1,128)} %bitcast.6, f32[1,512]{1,0:T(1,128)} %bitcast.7, bf16[512,2048]{1,0:T(8,128)(2,1)} %proj_hbm.1, bf16[64,2048]{1,0:T(8,128)(2,1)} %mi_hbm.1, ...), custom_call_target="tpu_custom_call" | custom-call | tf_op jit(solution)/shard_map/pallas_call | solution.py:476
  111.2 1.0 copy.16
  112.2 0.7 copy.17

commit v4 on v3

--- a/solution.py
+++ b/solution.py
@@ -294,7 +294,7 @@
 
     lane = lax.broadcasted_iota(jnp.int32, (RB, 128), 1)
 
-    def conv_rows(rb, stats):
+    def conv_rows(rb, carry):
         base = pl.multiple_of(rb * RB, RB)
         total = jnp.zeros((RB, 128), F32)
         squares = jnp.zeros((RB, 128), F32)
@@ -305,39 +305,59 @@
             mixed[cb, pl.ds(base, RB), :] = acc
             total = total + acc
             squares = squares + acc * acc
-        stats = jnp.where(lane == rb, jnp.sum(total, axis=1, keepdims=True), stats)
-        return jnp.where(lane == rb + NRB, jnp.sum(squares, axis=1, keepdims=True), stats)
-
-    stats = lax.fori_loop(1, NRB // 2, conv_rows, jnp.zeros((RB, 128), F32))
-    dispatch(2)
-    dispatch(3)
-    gather_start(0)
-    dispatch(4)
-    share_yy()
-    @pl.when(g > 0)
-    def _():
-        halo.wait_recv()
-
-    @pl.when(g == 0)
-    def _():
-        xb[0:HALO, :] = jnp.zeros((HALO, BLK), BF16)
-
-    for cb in range(NCB):
-        xf[cb, 0:HALO, :] = xb[0:HALO, cb * 128 : cb * 128 + 128].astype(F32)
-    stats = lax.fori_loop(NRB // 2, NRB, conv_rows, stats)
-    stats = conv_rows(0, stats)
-    tst[TP] = stats
+        stats = jnp.where(lane == rb, jnp.sum(total, axis=1, keepdims=True), tst[TP])
+        tst[TP] = jnp.where(lane == rb + NRB, jnp.sum(squares, axis=1, keepdims=True), stats)
+        return carry
+
+    def conv_span(first, last):
+        lax.fori_loop(first, last, conv_rows, 0)
+
+    def conv_last():
+        @pl.when(g > 0)
+        def _():
+            halo.wait_recv()
+
+        @pl.when(g == 0)
+        def _():
+            xb[0:HALO, :] = jnp.zeros((HALO, BLK), BF16)
+
+        for cb in range(NCB):
+            xf[cb, 0:HALO, :] = xb[0:HALO, cb * 128 : cb * 128 + 128].astype(F32)
+        conv_span(0, 1)
+        for d in range(1, TP):
+            to = (y + d) % TP
+            stat_sends.append(remote(tst.at[TP], tst.at[y], st_send.at[d], st_recv.at[d], g, to))
+            stat_sends[-1].start()
+
+    def activate_span(first, last):
+        means = (tst[TP] + tst[right] + tst[opp] + tst[left]) * (1.0 / D)
+
+        def activate(rb, carry):
+            base = pl.multiple_of(rb * RB, RB)
+            center = jnp.sum(jnp.where(lane == rb, means, 0.0), axis=1, keepdims=True)
+            square = jnp.sum(jnp.where(lane == rb + NRB, means, 0.0), axis=1, keepdims=True)
+            inv = lax.rsqrt(jnp.maximum(square - center * center, 0.0) + 1e-5)
+            for cb in range(NCB):
+                cols = slice(cb * 128, cb * 128 + 128)
+                v = (mixed[cb, pl.ds(base, RB), :] - center) * inv * gain_ref[:, cols] + shift_ref[:, cols]
+                act[pl.ds(base, RB), cols] = (v / (1.0 + jnp.exp(-v))).astype(BF16)
+            return carry
+
+        lax.fori_loop(first, last, activate, 0)
+
+    def share_act(d):
+        to = (y + d) % TP
+        remote(
+            act.at[pl.ds(pl.multiple_of(to * QROWS, QROWS), QROWS)],
+            actf.at[:, pl.ds(ycol, BLK)],
+            act_send,
+            act_recv.at[d],
+            g,
+            to,
+        ).start()
+
     stat_sends = []
-    for d in range(1, TP):
-        to = (y + d) % TP
-        stat_sends.append(remote(tst.at[TP], tst.at[y], st_send.at[d], st_recv.at[d], g, to))
-        stat_sends[-1].start()
-
-    gather_forward(0)
-    gather_start(1)
-    dispatch(5)
-    dispatch(6)
-    dispatch(7)
+    tst[TP] = jnp.zeros((RB, 128), F32)
     pick = lax.broadcasted_iota(jnp.int32, (128, GROUP), 0)
     table = jnp.where(pick == 0, rt_ref[0:1, :].astype(F32), 0.0)
     table = jnp.where(pick == 1, rt_ref[1:2, :].astype(F32), table)
@@ -362,54 +382,49 @@
     whi[...] = jnp.where(hit, jnp.dot(weight_hi, spread_cols, preferred_element_type=F32), 0.0).astype(BF16)
     wlo[...] = jnp.where(hit, jnp.dot(weight_lo, spread_cols, preferred_element_type=F32), 0.0).astype(BF16)
 
-    for d in range(1, TP):
-        landed(tst.at[0], st_recv.at[d])
-    means = (tst[TP] + tst[right] + tst[opp] + tst[left]) * (1.0 / D)
-
-    def activate(rb, carry):
-        base = pl.multiple_of(rb * RB, RB)
-        center = jnp.sum(jnp.where(lane == rb, means, 0.0), axis=1, keepdims=True)
-        square = jnp.sum(jnp.where(lane == rb + NRB, means, 0.0), axis=1, keepdims=True)
-        inv = lax.rsqrt(jnp.maximum(square - center * center, 0.0) + 1e-5)
-        for cb in range(NCB):
-            cols = slice(cb * 128, cb * 128 + 128)
-            v = (mixed[cb, pl.ds(base, RB), :] - center) * inv * gain_ref[:, cols] + shift_ref[:, cols]
-            act[pl.ds(base, RB), cols] = (v / (1.0 + jnp.exp(-v))).astype(BF16)
-        return carry
-
-    lax.fori_loop(0, NRB, activate, 0)
-    def share_act(d):
-        to = (y + d) % TP
-        remote(
-            act.at[pl.ds(pl.multiple_of(to * QROWS, QROWS), QROWS)],
-            actf.at[:, pl.ds(ycol, BLK)],
-            act_send,
-            act_recv.at[d],
-            g,
-            to,
-        ).start()
-
-    actf[:, pl.ds(ycol, BLK)] = act[pl.ds(pl.multiple_of(y * QROWS, QROWS), QROWS), :]
-
+    conv_span(1, 4)
+    gather_start(0)
+    dispatch(2)
+    dispatch(3)
+    dispatch(4)
+    share_yy()
+    gather_forward(0)
+    gather_start(1)
+    dispatch(5)
+    dispatch(6)
+    dispatch(7)
     for load in loads[3:]:
         load.wait()
-    share_x()
+    conv_span(4, 6)
     for k in range(NCH):
         experts(k)
         if k + 1 < NCH:
             gather_forward(k + 1)
         if k + 2 < NCH:
             gather_start(k + 2)
+        if k == 0:
+            share_x()
         if k >= 1:
             give_back(k - 1)
+        if k < 3:
+            conv_span(6 + 3 * k, 9 + 3 * k)
+        if k == 3:
+            conv_span(15, 16)
+            conv_last()
         if k == NCH - 3:
             share_xx()
+            for d in range(1, TP):
+                landed(tst.at[0], st_recv.at[d])
+            activate_span(0, NRB // 2)
+        if k == NCH - 2:
+            activate_span(NRB // 2, NRB)
         if k == NCH - 1:
             share_core()
     give_back(NCH - 1)
     share_act(2)
     share_act(1)
     share_act(3)
+    actf[:, pl.ds(ycol, BLK)] = act[pl.ds(pl.multiple_of(y * QROWS, QROWS), QROWS), :]
 
     def combine(rows):
         total = jnp.dot(whi[...], rows[...], preferred_element_type=F32)

time: 113 us -> 112 us (level)
  Pallas kernels: 111 us -> 109 us
    pallas_call x1, Pallas kernels: 111 us -> 109 us  [local(): pl.pallas_call(kernel, out_shape=(pltpu.VMEM((QROWS, D), BF16), pltpu.VME...]
where the time goes in v4:
time: 112 us
  Pallas kernels  109 us (97%)
  local copies, waits for them, and re-layouts  1.67 us (1%)
    pallas_call x1, Pallas kernels, local(): pl.pallas_call(kernel, out_shape=(pltpu.VMEM((QROWS, D), BF16), pltpu.VME...  109 us

profile of v4, /device:TPU:8, one launch (start us, length us, event | category | flops | bytes accessed | tf_op | source)
XLA Modules:
  0.0 111.6 jit_solution(13353605803946591042)
XLA Ops:
  0.6 109.3 %shard_map.131 = (bf16[256,2048]{1,0:T(8,128)(2,1)S(1)}, bf16[64,2048]{1,0:T(8,128)(2,1)S(1)}) custom-call(bf16[1024,512]{1,0:T(8,128)(2,1)} %x_hbm.1, bf16[31,512]{1,0:T(8,128)(2,1)} %ck_ref.1, f32[1,512]{1,0:T(1,128)} %bitcast.6, f32[1,512]{1,0:T(1,128)} %bitcast.7, bf16[512,2048]{1,0:T(8,128)(2,1)} %proj_hbm.1, bf16[64,2048]{1,0:T(8,128)(2,1)} %mi_hbm.1, ...), custom_call_target="tpu_custom_call" | custom-call | tf_op jit(solution)/shard_map/pallas_call | solution.py:491
  110.0 1.0 copy.16
  110.9 0.7 copy.17
